TPU v7x, 32 devices: a whole 2x2x4 slice. The times are simulated.
32 devices in a mesh: grp: 2 (over x), fs: 4 (over z), tp: 4 (over y, core).
Axes of the slice: x: 2, y: 2, z: 4, core: 2. Of those that a mesh axis runs over, the one named last changes fastest.
Arguments:
- tokens: bfloat16 [2048, 2048], P(('grp', 'fs'), 'tp'), parts along dimension 0, may hold values from -12 to 12
- gain_first: float32 [2048], P('tp'), may hold values from 0.1 to 1.9
- gate_first: float32 [2048, 5632], P('fs', 'tp'), may hold values from -0.125 to 0.125
- gate_scale_first: float32 [5632], P('tp'), may hold values from 0.5 to 2
- up_first: float32 [2048, 5632], P('fs', 'tp'), may hold values from -0.125 to 0.125
- up_scale_first: float32 [5632], P('tp'), may hold values from 0.5 to 2
- down_first: float32 [5632, 2048], P('tp', 'fs'), may hold values from -0.078125 to 0.078125
- down_scale_first: float32 [2048], P('tp'), may hold values from 0.5 to 2
- gain_second: float32 [2048], P('tp'), may hold values from 0.1 to 1.9
- gate_second: float32 [2048, 5632], P('fs', 'tp'), may hold values from -0.125 to 0.125
- gate_scale_second: float32 [5632], P('tp'), may hold values from 0.5 to 2
- up_second: float32 [2048, 5632], P('fs', 'tp'), may hold values from -0.125 to 0.125
- up_scale_second: float32 [5632], P('tp'), may hold values from 0.5 to 2
- down_second: float32 [5632, 2048], P('tp', 'fs'), may hold values from -0.078125 to 0.078125
- down_scale_second: float32 [2048], P('tp'), may hold values from 0.5 to 2
Outputs:
- stream_out: bfloat16 [2048, 2048], P(('grp', 'fs'), 'tp'), parts along dimension 0
There are 2 independent parts, one for each index of `grp`. A program takes and returns all parts, laid end to end along the dimension named above; an argument that names none is the same for every part. Nothing has to cross between parts.
All inputs are finite; a program needn't handle non-finite values.
Results may differ from a plain program's by a relative error of at most 0.028.
Values may be sent and summed in bfloat16 or wider, within the bound.
A program may use at most 128 MiB of HBM per device.

v0:
```python
import jax
import jax.numpy as jnp
from jax import lax
from jax.sharding import PartitionSpec as P

epsilon = 1e-06


def normalize(stream, gain):
    values = stream.astype(jnp.float32)
    totals = lax.psum(jnp.sum(values * values, axis=1), "tp")
    width = values.shape[1] * lax.axis_size("tp")
    normed = (values * lax.rsqrt(totals / width + epsilon)[:, None] * gain).astype(jnp.bfloat16)
    whole = lax.all_gather(normed, "tp", axis=1, tiled=True)
    return (values, whole)


def add_rows(whole, piece):
    return jnp.dot(whole, piece, preferred_element_type=jnp.float32)


def collect_gate_up(whole, gate_w, up_w):
    gate_bf = gate_w.astype(jnp.bfloat16)
    up_bf = up_w.astype(jnp.bfloat16)

    def add_one(piece):
        return add_rows(whole, piece)

    gate = add_one(lax.all_gather(gate_bf, "fs", axis=0, tiled=True))
    up = add_one(lax.all_gather(up_bf, "fs", axis=0, tiled=True))
    return (gate, up)


def collect_down(hidden, down_w):
    return jnp.dot(
        hidden,
        lax.all_gather(down_w.astype(jnp.bfloat16), "fs", axis=1, tiled=True),
        preferred_element_type=jnp.float32,
    )


def finish(values, gate, up, gate_s, up_s, down_s, down_fn):
    hidden = (jax.nn.silu(gate * gate_s) * (up * up_s)).astype(jnp.bfloat16)
    terms = down_fn(hidden)
    summed = lax.psum_scatter(
        terms.astype(jnp.bfloat16), "tp", scatter_dimension=1, tiled=True
    ).astype(jnp.float32)
    return (values + 0.5 * summed * down_s).astype(jnp.bfloat16)


def body(
    tokens,
    gain_first,
    gate_first,
    gate_scale_first,
    up_first,
    up_scale_first,
    down_first,
    down_scale_first,
    gain_second,
    gate_second,
    gate_scale_second,
    up_second,
    up_scale_second,
    down_second,
    down_scale_second,
):
    values, whole = normalize(tokens, gain_first)
    gate, up = collect_gate_up(whole, gate_first, up_first)
    middle = finish(
        values,
        gate,
        up,
        gate_scale_first,
        up_scale_first,
        down_scale_first,
        lambda hidden: collect_down(hidden, down_first),
    )
    values, whole = normalize(middle, gain_second)
    gate, up = collect_gate_up(whole, gate_second, up_second)
    return finish(
        values,
        gate,
        up,
        gate_scale_second,
        up_scale_second,
        down_scale_second,
        lambda hidden: collect_down(hidden, down_second),
    )


def solution(mesh):
    in_specs = (
        P(("grp", "fs"), "tp"),
        P("tp"),
        P("fs", "tp"),
        P("tp"),
        P("fs", "tp"),
        P("tp"),
        P("tp", "fs"),
        P("tp"),
        P("tp"),
        P("fs", "tp"),
        P("tp"),
        P("fs", "tp"),
        P("tp"),
        P("tp", "fs"),
        P("tp"),
    )
    out_specs = P(("grp", "fs"), "tp")
    return jax.shard_map(body, mesh=mesh, in_specs=in_specs, out_specs=out_specs, check_vma=False)
```

profile of v0, /device:TPU:0, one launch (start us, length us, event | category | flops | bytes accessed | tf_op | source)
XLA Modules:
  0.0 769.3 jit_solution(5649836803624989204)
XLA Ops:
  6.5 0.0 all-gather.9.cloned.1.call-start
  6.5 1.1 fusion.4
  7.6 8.4 %psum.14 = f32[256]{0:T(256)S(1)} all-reduce(f32[256]{0:T(256)S(1)} %fusion.4), channel_id=1, replica_groups=mesh['grp'=2,'fs'=4,'tp'=4] {'tp'}, use_global_device_ids=true, to_apply=%region_1.0 | all-reduce | flops 256 | bytes 2048 | tf_op jit(solution)/shard_map/psum | solution.py:11
  16.0 1.8 fusion.6
  17.8 0.0 all-gather.9.cloned.1.call-update
  17.8 0.0 all-gather.11.cloned.1.call-start
  17.9 0.0 copy-start
  17.9 3.3 convert_element_type.56
  21.2 0.0 all-gather.11.cloned.1.call-update
  21.2 0.0 all-gather.13.cloned.1.call-start
  21.2 0.0 copy-done
  21.2 1.3 convert_element_type.57
  22.5 0.0 all-gather.13.cloned.1.call-update
  22.5 0.0 all-gather.15.cloned.1.call-start
  22.6 3.2 convert_element_type.59
  25.8 0.0 all-gather.15.cloned.1.call-update
  25.8 0.0 copy-start.9
  25.8 0.0 reduce-scatter.3.cloned.1.call-start
  25.8 9.1 %all-gather.9.cloned.1.call-done = bf16[256,2048]{1,0:T(8,128)(2,1)} async-done(((bf16[256,512]{1,0:T(8,128)(2,1)}), bf16[256,2048]{1,0:T(8,128)(2,1)}) %all-gather.9.cloned.1.call-update) | async-done | bytes 1048592 | tf_op jit(solution)/shard_map/all_gather | solution.py:14
  35.0 108.3 %all-gather.11.cloned.1.call-done = bf16[2048,1408]{1,0:T(8,128)(2,1)} async-done(((bf16[512,1408]{1,0:T(8,128)(2,1)}), bf16[2048,1408]{1,0:T(8,128)(2,1)}) %all-gather.11.cloned.1.call-update) | async-done | bytes 5767184 | tf_op jit(solution)/shard_map/all_gather | solution.py:29
  143.3 0.0 copy-done.8
  143.3 5.9 convolution_multiply_fusion.3
  149.2 100.6 %all-gather.13.cloned.1.call-done = bf16[2048,1408]{1,0:T(8,128)(2,1)} async-done(((bf16[512,1408]{1,0:T(8,128)(2,1)}), bf16[2048,1408]{1,0:T(8,128)(2,1)}) %all-gather.13.cloned.1.call-update) | async-done | bytes 5767184 | tf_op jit(solution)/shard_map/all_gather | solution.py:30
  249.8 106.4 %all-gather.15.cloned.1.call-done = bf16[1408,2048]{1,0:T(8,128)(2,1)} async-done(((bf16[1408,512]{1,0:T(8,128)(2,1)}), bf16[1408,2048]{1,0:T(8,128)(2,1)}) %all-gather.15.cloned.1.call-update) | async-done | bytes 5767184 | tf_op jit(solution)/shard_map/all_gather | solution.py:37
  356.2 0.0 copy-done.9
  356.2 9.6 %convolution_convert_fusion.1 = bf16[256,2048]{1,0:T(8,128)(2,1)} fusion(bf16[1408,2048]{1,0:T(8,128)(2,1)} %all-gather.15.cloned.1.call-done, bf16[256,2048]{1,0:T(8,128)(2,1)} %all-gather.9.cloned.1.call-done, bf16[2048,1408]{1,0:T(8,128)(2,1)} %all-gather.13.cloned.1.call-done, f32[256,1408]{1,0:T(8,128)} %convolution_multiply_fusion.3, ...), kind=kOutput, calls=%fused_computation.9 | convolution fusion | flops 2955837440 | bytes 15078912 | tf_op jit(solution)/shard_map/dot_general | solution.py:35
  365.9 0.0 reduce-scatter.3.cloned.1.call-update
  365.9 0.0 all-gather.19.cloned.1.call-start
  365.9 0.0 copy-done.1
  366.0 0.0 copy-start.3
  366.0 1.3 convert_element_type.65
  367.3 0.0 all-gather.19.cloned.1.call-update
  367.3 0.0 all-gather.17.cloned.1.call-start
  367.3 0.6 copy-done.5
  367.9 21.1 %reduce-scatter.3.cloned.1.call-done = bf16[256,512]{1,0:T(8,128)(2,1)} async-done(((bf16[256,2048]{1,0:T(8,128)(2,1)}), bf16[256,512]{1,0:T(8,128)(2,1)}) %reduce-scatter.3.cloned.1.call-update) | async-done | bytes 262160 | tf_op jit(solution)/shard_map/reduce_scatter | solution.py:45
  389.1 0.0 copy-done.3
  389.1 1.1 fusion.8
  390.2 5.8 psum.15
  396.0 0.0 copy-done.4
  396.0 0.8 fusion.10
  396.8 0.0 all-gather.17.cloned.1.call-update
  396.9 0.0 all-gather.21.cloned.1.call-start
  396.9 0.0 copy-done.2
  396.9 1.3 convert_element_type.66
  398.2 0.0 all-gather.21.cloned.1.call-update
  398.2 0.0 all-gather.23.cloned.1.call-start
  398.3 3.4 convert_element_type.68
  401.7 0.0 all-gather.23.cloned.1.call-update
  401.7 0.0 copy-start.11
  401.7 0.0 reduce-scatter.5.cloned.1.call-start
  401.8 95.4 %all-gather.19.cloned.1.call-done = bf16[2048,1408]{1,0:T(8,128)(2,1)} async-done(((bf16[512,1408]{1,0:T(8,128)(2,1)}), bf16[2048,1408]{1,0:T(8,128)(2,1)}) %all-gather.19.cloned.1.call-update) | async-done | bytes 5767184 | tf_op jit(solution)/shard_map/all_gather | solution.py:29
  497.2 16.6 %all-gather.17.cloned.1.call-done = bf16[256,2048]{1,0:T(8,128)(2,1)} async-done(((bf16[256,512]{1,0:T(8,128)(2,1)}), bf16[256,2048]{1,0:T(8,128)(2,1)}) %all-gather.17.cloned.1.call-update) | async-done | bytes 1048592 | tf_op jit(solution)/shard_map/all_gather | solution.py:14
  513.8 0.0 copy-done.10
  513.8 4.8 convolution_multiply_fusion.1
  518.7 0.0 copy-start.6
  518.7 103.4 %all-gather.21.cloned.1.call-done = bf16[2048,1408]{1,0:T(8,128)(2,1)} async-done(((bf16[512,1408]{1,0:T(8,128)(2,1)}), bf16[2048,1408]{1,0:T(8,128)(2,1)}) %all-gather.21.cloned.1.call-update) | async-done | bytes 5767184 | tf_op jit(solution)/shard_map/all_gather | solution.py:30
  622.1 106.5 %all-gather.23.cloned.1.call-done = bf16[1408,2048]{1,0:T(8,128)(2,1)} async-done(((bf16[1408,512]{1,0:T(8,128)(2,1)}), bf16[1408,2048]{1,0:T(8,128)(2,1)}) %all-gather.23.cloned.1.call-update) | async-done | bytes 5767184 | tf_op jit(solution)/shard_map/all_gather | solution.py:37
  728.7 0.0 copy-done.11
  728.7 0.0 copy-done.7
  728.7 8.9 %convolution_convert_fusion = bf16[256,2048]{1,0:T(8,128)(2,1)} fusion(bf16[1408,2048]{1,0:T(8,128)(2,1)} %all-gather.23.cloned.1.call-done, bf16[256,2048]{1,0:T(8,128)(2,1)S(1)} %copy-done.7, bf16[2048,1408]{1,0:T(8,128)(2,1)} %all-gather.21.cloned.1.call-done, f32[256,1408]{1,0:T(8,128)S(1)} %convolution_multiply_fusion.1, f32[1408]{0:T(1024)S(1)} %copy-done.11), kind=kOutput, calls=%fused_computation.8 | convolution fusion | flops 2955837440 | bytes 15078912 | tf_op jit(solution)/shard_map/dot_general | solution.py:35
  737.5 0.0 reduce-scatter.5.cloned.1.call-update
  737.5 0.0 copy-done.6
  737.6 23.2 %reduce-scatter.5.cloned.1.call-done = bf16[256,512]{1,0:T(8,128)(2,1)} async-done(((bf16[256,2048]{1,0:T(8,128)(2,1)}), bf16[256,512]{1,0:T(8,128)(2,1)}) %reduce-scatter.5.cloned.1.call-update) | async-done | bytes 262160 | tf_op jit(solution)/shard_map/reduce_scatter | solution.py:45
  760.7 1.7 fusion.11
  (11 shorter events, 0.0 us)
Async XLA Ops:
  6.5 28.5 %all-gather.9.cloned.1.call-start = ((), (), s32[]{:S(2)}) async-start(), calls=%async_computation.2 | async-start | bytes 1310720 | tf_op jit(solution)/shard_map/all_gather | solution.py:14
  17.8 125.4 %all-gather.11.cloned.1.call-start = ((), (), s32[]{:S(2)}) async-start(), calls=%async_computation.3 | async-start | bytes 7208960 | tf_op jit(solution)/shard_map/all_gather | solution.py:29
  17.9 3.3 copy-start
  21.2 228.6 %all-gather.13.cloned.1.call-start = ((), (), s32[]{:S(2)}) async-start(), calls=%async_computation.4 | async-start | bytes 7208960 | tf_op jit(solution)/shard_map/all_gather | solution.py:30
  22.5 333.7 %all-gather.15.cloned.1.call-start = ((), (), s32[]{:S(2)}) async-start(), calls=%async_computation.5 | async-start | bytes 7208960 | tf_op jit(solution)/shard_map/all_gather | solution.py:37
  25.8 117.5 %copy-start.8 = (f32[1408]{0:T(1024)S(1)}, f32[1408]{0:T(1024)}, u32[]{:S(2)}) copy-start(f32[1408]{0:T(1024)} %param.18) | copy-start | bytes 16900
  25.8 330.5 %copy-start.9 = (f32[1408]{0:T(1024)S(1)}, f32[1408]{0:T(1024)}, u32[]{:S(2)}) copy-start(f32[1408]{0:T(1024)} %param.20) | copy-start | bytes 16900
  25.8 363.3 %reduce-scatter.3.cloned.1.call-start = ((), (), s32[]{:S(2)}) async-start(), calls=%async_computation.6 | async-start | bytes 1310720 | tf_op jit(solution)/shard_map/reduce_scatter | solution.py:45
  356.2 9.7 %copy-start.1 = (f32[512,1408]{1,0:T(8,128)S(1)}, f32[512,1408]{1,0:T(8,128)}, u32[]{:S(2)}) copy-start(f32[512,1408]{1,0:T(8,128)} %param.24) | copy-start | bytes 8650756
  365.9 131.3 %all-gather.19.cloned.1.call-start = ((), (), s32[]{:S(2)}) async-start(), calls=%async_computation.8 | async-start | bytes 7208960 | tf_op jit(solution)/shard_map/all_gather | solution.py:29
  366.0 23.1 %copy-start.3 = (bf16[256,512]{1,0:T(8,128)(2,1)S(1)}, bf16[256,512]{1,0:T(8,128)(2,1)}, u32[]{:S(2)}) copy-start(bf16[256,512]{1,0:T(8,128)(2,1)} %param.15) | copy-start | bytes 786436
  367.3 0.7 copy-start.5
  367.3 28.7 %copy-start.4 = (f32[512]{0:T(512)S(1)}, f32[512]{0:T(512)}, u32[]{:S(2)}) copy-start(f32[512]{0:T(512)} %param.23) | copy-start | bytes 6148
  367.3 29.6 %copy-start.2 = (f32[512,1408]{1,0:T(8,128)S(1)}, f32[512,1408]{1,0:T(8,128)}, u32[]{:S(2)}) copy-start(f32[512,1408]{1,0:T(8,128)} %param.26) | copy-start | bytes 8650756
  367.3 146.5 %all-gather.17.cloned.1.call-start = ((), (), s32[]{:S(2)}) async-start(), calls=%async_computation.7 | async-start | bytes 1310720 | tf_op jit(solution)/shard_map/all_gather | solution.py:14
  396.9 225.2 %all-gather.21.cloned.1.call-start = ((), (), s32[]{:S(2)}) async-start(), calls=%async_computation.9 | async-start | bytes 7208960 | tf_op jit(solution)/shard_map/all_gather | solution.py:30
  398.2 330.4 %all-gather.23.cloned.1.call-start = ((), (), s32[]{:S(2)}) async-start(), calls=%async_computation.10 | async-start | bytes 7208960 | tf_op jit(solution)/shard_map/all_gather | solution.py:37
  401.7 112.1 %copy-start.10 = (f32[1408]{0:T(1024)S(1)}, f32[1408]{0:T(1024)}, u32[]{:S(2)}) copy-start(f32[1408]{0:T(1024)} %param.25) | copy-start | bytes 16900
  401.7 326.9 %copy-start.11 = (f32[1408]{0:T(1024)S(1)}, f32[1408]{0:T(1024)}, u32[]{:S(2)}) copy-start(f32[1408]{0:T(1024)} %param.27) | copy-start | bytes 16900
  401.7 359.0 %reduce-scatter.5.cloned.1.call-start = ((), (), s32[]{:S(2)}) async-start(), calls=%async_computation.11 | async-start | bytes 1310720 | tf_op jit(solution)/shard_map/reduce_scatter | solution.py:45
  513.8 214.8 %copy-start.7 = (bf16[256,2048]{1,0:T(8,128)(2,1)S(1)}, bf16[256,2048]{1,0:T(8,128)(2,1)}, u32[]{:S(2)}) copy-start(bf16[256,2048]{1,0:T(8,128)(2,1)} %all-gather.17.cloned.1.call-done) | copy-start | bytes 3145732
  518.7 218.9 %copy-start.6 = (f32[512]{0:T(512)S(1)}, f32[512]{0:T(512)}, u32[]{:S(2)}) copy-start(f32[512]{0:T(512)} %param.29) | copy-start | bytes 6148
Sparse Core Ops, SparseCore 0:
  18.0 16.9 all-gather.8
  36.6 106.6 all-gather.10
  144.9 104.9 all-gather.12
  251.3 104.9 all-gather.14
  366.0 23.0 reduce-scatter.2
  390.5 106.6 all-gather.18
  498.8 14.9 all-gather.16
  515.4 106.6 all-gather.20
  623.7 104.9 all-gather.22
  737.7 23.0 reduce-scatter.4
where the time goes:
time: 770 us; the launch traced here: 769 us
  waiting for transfers between devices  691 us (90%)
  matrix products  29.2 us (4%)
  other arithmetic  20.3 us (3%)
  blocking collectives  14.2 us (2%)
  between operations  13.6 us (2%)
    all_gather x2, waiting for transfers between devices, collect_down(): lax.all_gather(down_w.astype(jnp.bfloat16), 'fs', axis=1, tiled=True)  213 us
    all_gather x2, waiting for transfers between devices, collect_gate_up(): up = add_one(lax.all_gather(up_bf, 'fs', axis=0, tiled=True))  204 us
    all_gather x2, waiting for transfers between devices, collect_gate_up(): gate = add_one(lax.all_gather(gate_bf, 'fs', axis=0, tiled=True))  204 us
    reduce_scatter x2, waiting for transfers between devices, finish(): lax.psum_scatter(terms.astype(jnp.bfloat16), 'tp', scatter_dimension=1, t...  44.3 us
    all_gather x2, waiting for transfers between devices, normalize(): whole = lax.all_gather(normed, 'tp', axis=1, tiled=True)  25.7 us
    dot_general x2, matrix products, collect_down(): jnp.dot(hidden, lax.all_gather(down_w.astype(jnp.bfloat16), 'fs', axis=1,...  18.5 us
  transfers between devices with their start and end apart: 10, of which 10 were waited for; matrix products, arithmetic and copies ran while one was open for 3% of the time, Pallas kernels for 0%

commit v1 on v0

--- a/solution.py
+++ b/solution.py
@@ -48,7 +48,7 @@
     return (values + 0.5 * summed * down_s).astype(jnp.bfloat16)
 
 
-def body(
+def body_gather(
     tokens,
     gain_first,
     gate_first,
@@ -89,6 +89,65 @@
     )
 
 
+def reshard_columns(weight):
+    return lax.all_to_all(weight.astype(jnp.bfloat16), "fs", 1, 0, tiled=True)
+
+
+def reshard_rows(weight):
+    return lax.all_to_all(weight.astype(jnp.bfloat16), "fs", 0, 1, tiled=True)
+
+
+def own_columns(scale):
+    width = scale.shape[0] // lax.axis_size("fs")
+    return lax.dynamic_slice_in_dim(scale, lax.axis_index("fs") * width, width)
+
+
+def block(stream, gain, gate_w, gate_s, up_w, up_s, down_w, down_s):
+    values, whole = normalize(stream, gain)
+    every = lax.all_gather(whole, "fs", axis=0, tiled=True)
+    gate = jnp.dot(every, gate_w, preferred_element_type=jnp.float32) * own_columns(gate_s)
+    up = jnp.dot(every, up_w, preferred_element_type=jnp.float32) * own_columns(up_s)
+    hidden = (jax.nn.silu(gate) * up).astype(jnp.bfloat16)
+    terms = jnp.dot(hidden, down_w, preferred_element_type=jnp.float32).astype(jnp.bfloat16)
+    mine = lax.psum_scatter(terms, "tp", scatter_dimension=1, tiled=True)
+    summed = lax.psum_scatter(mine, "fs", scatter_dimension=0, tiled=True).astype(jnp.float32)
+    return (values + 0.5 * summed * down_s).astype(jnp.bfloat16)
+
+
+def body_reshard(
+    tokens,
+    gain_first,
+    gate_first,
+    gate_scale_first,
+    up_first,
+    up_scale_first,
+    down_first,
+    down_scale_first,
+    gain_second,
+    gate_second,
+    gate_scale_second,
+    up_second,
+    up_scale_second,
+    down_second,
+    down_scale_second,
+):
+    weights = [
+        (reshard_columns(gate), reshard_columns(up), reshard_rows(down))
+        for gate, up, down in (
+            (gate_first, up_first, down_first),
+            (gate_second, up_second, down_second),
+        )
+    ]
+    gate_w, up_w, down_w = weights[0]
+    middle = block(
+        tokens, gain_first, gate_w, gate_scale_first, up_w, up_scale_first, down_w, down_scale_first
+    )
+    gate_w, up_w, down_w = weights[1]
+    return block(
+        middle, gain_second, gate_w, gate_scale_second, up_w, up_scale_second, down_w, down_scale_second
+    )
+
+
 def solution(mesh):
     in_specs = (
         P(("grp", "fs"), "tp"),
@@ -108,4 +167,8 @@
         P("tp"),
     )
     out_specs = P(("grp", "fs"), "tp")
+    def body(*args):
+        width = args[2].shape[1] // lax.axis_size("fs")
+        return (body_reshard if width >= 128 else body_gather)(*args)
+
     return jax.shard_map(body, mesh=mesh, in_specs=in_specs, out_specs=out_specs, check_vma=False)

time: 770 us -> 555 us (0.72)
  waiting for transfers between devices: 691 us -> 429 us
  starting transfers between devices: 0.38 us -> 32.7 us
  local copies, waits for them, and re-layouts: 0.66 us -> 22.4 us
    all_gather x6 -> x2, waiting for transfers between devices: 621 us -> 0.01 us  [block(): every = lax.all_gather(whole, 'fs', axis=0, tiled=True)]
    all_to_all x0 -> x6, waiting for transfers between devices: none -> 264 us  [the longest x4 204 us: reshard_columns(): return lax.all_to_all(weight.astype(jnp.bfloat16), 'fs', 1, 0, tiled=True)]
    reduce_scatter x2 -> x4, waiting for transfers between devices: 44.3 us -> 146 us  [the longest x2 87.1 us: block(): mine = lax.psum_scatter(terms, 'tp', scatter_dimension=1, tiled=True)]
    all_to_all x0 -> x6, starting transfers between devices: none -> 32.3 us  [the longest x4 23.4 us: reshard_columns(): return lax.all_to_all(weight.astype(jnp.bfloat16), 'fs', 1, 0, tiled=True)]
    unnamed x24 -> x18, local copies, waits for them, and re-layouts: 0.66 us -> 10.6 us
    all_to_all x0 -> x6, local copies, waits for them, and re-layouts: none -> 8.68 us  [the longest x2 5.65 us: reshard_rows(): return lax.all_to_all(weight.astype(jnp.bfloat16), 'fs', 0, 1, tiled=True)]
    convert_element_type x7 -> x3, other arithmetic: 15.4 us -> 8.14 us  [the longest x2 6.41 us: reshard_rows(): return lax.all_to_all(weight.astype(jnp.bfloat16), 'fs', 0, 1, tiled=True)]
  transfers between devices with their start and end apart: 10 -> 14, of which waited for: 10 -> 12; matrix products, arithmetic and copies ran while one was open for 3% -> 5% of each run, Pallas kernels for 0% -> 0%
where the time goes in v1:
time: 555 us; the launch traced here: 554 us
  waiting for transfers between devices  429 us (77%)
  starting transfers between devices  32.7 us (6%)
  matrix products  27.9 us (5%)
  local copies, waits for them, and re-layouts  22.4 us (4%)
  blocking collectives  14.6 us (3%)
  between operations  13.6 us (2%)
  other arithmetic  13 us (2%)
    all_to_all x4, waiting for transfers between devices, reshard_columns(): return lax.all_to_all(weight.astype(jnp.bfloat16), 'fs', 1, 0, tiled=True)  204 us
    reduce_scatter x2, waiting for transfers between devices, block(): mine = lax.psum_scatter(terms, 'tp', scatter_dimension=1, tiled=True)  87.1 us
    all_to_all x2, waiting for transfers between devices, reshard_rows(): return lax.all_to_all(weight.astype(jnp.bfloat16), 'fs', 0, 1, tiled=True)  59.7 us
    reduce_scatter x2, waiting for transfers between devices, block(): lax.psum_scatter(mine, 'fs', scatter_dimension=0, tiled=True)  58.9 us
    all_to_all x4, starting transfers between devices, reshard_columns(): return lax.all_to_all(weight.astype(jnp.bfloat16), 'fs', 1, 0, tiled=True)  23.4 us
    all_gather x2, waiting for transfers between devices, normalize(): whole = lax.all_gather(normed, 'tp', axis=1, tiled=True)  19.1 us
    dot_general x2, matrix products, block(): jnp.dot(hidden, down_w, preferred_element_type=jnp.float32)  18 us
    psum x2, blocking collectives, normalize(): totals = lax.psum(jnp.sum(values * values, axis=1), 'tp')  14.6 us
  transfers between devices with their start and end apart: 14, of which 12 were waited for; matrix products, arithmetic and copies ran while one was open for 5% of the time, Pallas kernels for 0%

profile of v1, /device:TPU:0, one launch (start us, length us, event | category | flops | bytes accessed | tf_op | source)
XLA Modules:
  0.0 553.6 jit_solution(2125384160684016210)
XLA Ops:
  6.5 0.0 all-gather.5.cloned.1.call-start
  6.5 1.1 fusion.8
  7.6 8.4 %psum.14 = f32[256]{0:T(256)S(1)} all-reduce(f32[256]{0:T(256)S(1)} %fusion.8), channel_id=1, replica_groups=mesh['grp'=2,'fs'=4,'tp'=4] {'tp'}, use_global_device_ids=true, to_apply=%region_1.0 | all-reduce | flops 256 | bytes 2048 | tf_op jit(solution)/shard_map/psum | solution.py:11
  16.0 1.8 fusion.10
  17.8 0.0 all-gather.5.cloned.1.call-update
  17.8 3.0 copy.26
  20.8 4.9 all-to-all-start
  25.7 0.0 all-gather.7.cloned.1.call-start
  25.7 9.3 %all-gather.5.cloned.1.call-done = bf16[256,2048]{1,0:T(8,128)(2,1)} async-done(((bf16[256,512]{1,0:T(8,128)(2,1)}), bf16[256,2048]{1,0:T(8,128)(2,1)}) %all-gather.5.cloned.1.call-update) | async-done | bytes 1048592 | tf_op jit(solution)/shard_map/all_gather | solution.py:14
  35.0 0.0 all-gather.7.cloned.1.call-update
  35.0 3.0 copy.28
  38.0 45.4 %all-to-all-done = bf16[512,4,352]{0,2,1:T(8,128)(2,1)S(1)} async-done(((bf16[512,4,352]{0,2,1:T(8,128)(2,1)}), bf16[512,4,352]{0,2,1:T(8,128)(2,1)S(1)}, u32[]{:S(2)}, u32[]{:S(2)}) %all-to-all-start) | async-done | bytes 1441824 | tf_op jit(solution)/shard_map/all_to_all | solution.py:93
  83.4 8.8 %all-to-all-start.1 = ((bf16[512,4,352]{0,2,1:T(8,128)(2,1)}), bf16[512,4,352]{0,2,1:T(8,128)(2,1)S(1)}, u32[]{:S(2)}, u32[]{:S(2)}) async-start(bf16[512,4,352]{0,2,1:T(8,128)(2,1)} %bitcast.40), calls=%async_computation.1 | async-start | bytes 2883584 | tf_op jit(solution)/shard_map/all_to_all | solution.py:93
  92.3 3.2 convert_element_type.59
  95.5 55.2 %all-to-all-done.1 = bf16[512,4,352]{0,2,1:T(8,128)(2,1)S(1)} async-done(((bf16[512,4,352]{0,2,1:T(8,128)(2,1)}), bf16[512,4,352]{0,2,1:T(8,128)(2,1)S(1)}, u32[]{:S(2)}, u32[]{:S(2)}) %all-to-all-start.1) | async-done | bytes 1441824 | tf_op jit(solution)/shard_map/all_to_all | solution.py:93
  150.7 4.6 all-to-all-start.2
  155.2 0.0 reduce-scatter.5.cloned.1.call-start
  155.2 0.8 dynamic_slice.12
  156.0 0.8 dynamic_slice.13
  156.8 1.3 copy.36
  158.1 0.2 copy.37
  158.3 29.8 %all-to-all-done.2 = bf16[4,352,512]{2,1,0:T(8,128)(2,1)} async-done(((bf16[4,352,512]{2,1,0:T(8,128)(2,1)}), bf16[4,352,512]{2,1,0:T(8,128)(2,1)}, u32[]{:S(2)}, u32[]{:S(2)}) %all-to-all-start.2) | async-done | bytes 1441824 | tf_op jit(solution)/shard_map/all_to_all | solution.py:97
  188.2 2.8 copy.38
  191.0 5.0 convolution_multiply_fusion.3
  196.0 9.0 %convolution_convert_fusion.1 = bf16[1024,2048]{1,0:T(8,128)(2,1)} fusion(bf16[352,2048]{1,0:T(8,128)(2,1)} %bitcast.46, bf16[1024,2048]{1,0:T(8,128)(2,1)} %all-gather.7.cloned.1.call-done, bf16[2048,352]{0,1:T(8,128)(2,1)S(1)} %bitcast.42, f32[1024,352]{0,1:T(8,128)} %convolution_multiply_fusion.3, f32[352]{0:T(512)S(1)} %dynamic_slice.13), kind=kOutput, calls=%fused_computation.1 | convolution fusion | flops 2957410304 | bytes 12715392 | tf_op jit(solution)/shard_map/dot_general | solution.py:111
  205.0 0.0 reduce-scatter.5.cloned.1.call-update
  205.0 0.0 copy-start.4
  205.0 0.0 reduce-scatter.7.cloned.1.call-start
  205.1 43.6 %reduce-scatter.5.cloned.1.call-done = bf16[1024,512]{1,0:T(8,128)(2,1)} async-done(((bf16[1024,2048]{1,0:T(8,128)(2,1)}), bf16[1024,512]{1,0:T(8,128)(2,1)}) %reduce-scatter.5.cloned.1.call-update) | async-done | bytes 1048592 | tf_op jit(solution)/shard_map/reduce_scatter | solution.py:112
  248.7 0.0 reduce-scatter.7.cloned.1.call-update
  248.7 0.0 all-gather.9.cloned.1.call-start
  248.7 29.4 %reduce-scatter.7.cloned.1.call-done = bf16[256,512]{1,0:T(8,128)(2,1)} async-done(((bf16[1024,512]{1,0:T(8,128)(2,1)}), bf16[256,512]{1,0:T(8,128)(2,1)}) %reduce-scatter.7.cloned.1.call-update) | async-done | bytes 262160 | tf_op jit(solution)/shard_map/reduce_scatter | solution.py:113
  278.1 1.1 fusion.12
  279.3 6.2 %psum.15 = f32[256]{0:T(256)S(1)} all-reduce(f32[256]{0:T(256)S(1)} %get-tuple-element.5), channel_id=1, replica_groups=mesh['grp'=2,'fs'=4,'tp'=4] {'tp'}, use_global_device_ids=true, to_apply=%region_5.6 | all-reduce | flops 256 | bytes 2048 | tf_op jit(solution)/shard_map/psum | solution.py:11
  285.4 0.0 copy-done.4
  285.4 0.8 fusion.14
  286.3 0.0 all-gather.9.cloned.1.call-update
  286.3 1.7 copy.31
  288.0 3.6 all-to-all-start.3
  291.6 0.0 all-gather.11.cloned.1.call-start
  291.6 9.8 %all-gather.9.cloned.1.call-done = bf16[256,2048]{1,0:T(8,128)(2,1)} async-done(((bf16[256,512]{1,0:T(8,128)(2,1)}), bf16[256,2048]{1,0:T(8,128)(2,1)}) %all-gather.9.cloned.1.call-update) | async-done | bytes 1048592 | tf_op jit(solution)/shard_map/all_gather | solution.py:14
  301.4 0.0 all-gather.11.cloned.1.call-update
  301.4 3.0 copy.33
  304.4 45.9 %all-to-all-done.3 = bf16[512,4,352]{0,2,1:T(8,128)(2,1)S(1)} async-done(((bf16[512,4,352]{0,2,1:T(8,128)(2,1)}), bf16[512,4,352]{0,2,1:T(8,128)(2,1)S(1)}, u32[]{:S(2)}, u32[]{:S(2)}) %all-to-all-start.3) | async-done | bytes 1441824 | tf_op jit(solution)/shard_map/all_to_all | solution.py:93
  350.3 6.2 %all-to-all-start.4 = ((bf16[512,4,352]{0,2,1:T(8,128)(2,1)}), bf16[512,4,352]{0,2,1:T(8,128)(2,1)S(1)}, u32[]{:S(2)}, u32[]{:S(2)}) async-start(bf16[512,4,352]{0,2,1:T(8,128)(2,1)} %bitcast.41), calls=%async_computation.6 | async-start | bytes 2883584 | tf_op jit(solution)/shard_map/all_to_all | solution.py:93
  356.5 3.2 convert_element_type.68
  359.7 57.8 %all-to-all-done.4 = bf16[512,4,352]{0,2,1:T(8,128)(2,1)S(1)} async-done(((bf16[512,4,352]{0,2,1:T(8,128)(2,1)}), bf16[512,4,352]{0,2,1:T(8,128)(2,1)S(1)}, u32[]{:S(2)}, u32[]{:S(2)}) %all-to-all-start.4) | async-done | bytes 1441824 | tf_op jit(solution)/shard_map/all_to_all | solution.py:93
  417.5 4.3 all-to-all-start.5
  421.8 0.2 reduce-scatter.9.cloned.1.call-start
  422.1 0.8 dynamic_slice.14
  422.8 0.8 dynamic_slice.15
  423.6 1.3 copy.39
  424.9 0.2 copy.40
  425.1 29.9 %all-to-all-done.5 = bf16[4,352,512]{2,1,0:T(8,128)(2,1)} async-done(((bf16[4,352,512]{2,1,0:T(8,128)(2,1)}), bf16[4,352,512]{2,1,0:T(8,128)(2,1)}, u32[]{:S(2)}, u32[]{:S(2)}) %all-to-all-start.5) | async-done | bytes 1441824 | tf_op jit(solution)/shard_map/all_to_all | solution.py:97
  455.0 2.8 copy.41
  457.8 0.0 copy-done.3
  457.8 5.0 convolution_multiply_fusion.1
  462.8 9.0 %convolution_convert_fusion = bf16[1024,2048]{1,0:T(8,128)(2,1)} fusion(bf16[352,2048]{1,0:T(8,128)(2,1)} %bitcast.47, bf16[1024,2048]{1,0:T(8,128)(2,1)} %all-gather.11.cloned.1.call-done, bf16[2048,352]{0,1:T(8,128)(2,1)S(1)} %bitcast.43, f32[1024,352]{0,1:T(8,128)} %convolution_multiply_fusion.1, f32[352]{0:T(512)S(1)} %dynamic_slice.15), kind=kOutput, calls=%fused_computation | convolution fusion | flops 2957410304 | bytes 12715392 | tf_op jit(solution)/shard_map/dot_general | solution.py:111
  471.8 0.0 reduce-scatter.9.cloned.1.call-update
  471.8 0.0 reduce-scatter.11.cloned.1.call-start
  471.9 43.5 %reduce-scatter.9.cloned.1.call-done = bf16[1024,512]{1,0:T(8,128)(2,1)} async-done(((bf16[1024,2048]{1,0:T(8,128)(2,1)}), bf16[1024,512]{1,0:T(8,128)(2,1)}) %reduce-scatter.9.cloned.1.call-update) | async-done | bytes 1048592 | tf_op jit(solution)/shard_map/reduce_scatter | solution.py:112
  515.4 0.0 reduce-scatter.11.cloned.1.call-update
  515.4 29.6 %reduce-scatter.11.cloned.1.call-done = bf16[256,512]{1,0:T(8,128)(2,1)} async-done(((bf16[1024,512]{1,0:T(8,128)(2,1)}), bf16[256,512]{1,0:T(8,128)(2,1)}) %reduce-scatter.11.cloned.1.call-update) | async-done | bytes 262160 | tf_op jit(solution)/shard_map/reduce_scatter | solution.py:113
  545.0 1.7 fusion.15
  (17 shorter events, 0.0 us)
Async XLA Ops:
  6.5 28.5 %all-gather.5.cloned.1.call-start = ((), (), s32[]{:S(2)}) async-start(), calls=%async_computation.10 | async-start | bytes 1310720 | tf_op jit(solution)/shard_map/all_gather | solution.py:14
  20.8 62.6 %all-to-all-start = ((bf16[512,4,352]{0,2,1:T(8,128)(2,1)}), bf16[512,4,352]{0,2,1:T(8,128)(2,1)S(1)}, u32[]{:S(2)}, u32[]{:S(2)}) async-start(bf16[512,4,352]{0,2,1:T(8,128)(2,1)} %bitcast), calls=%async_computation | async-start | bytes 2883584 | tf_op jit(solution)/shard_map/all_to_all | solution.py:93
  25.7 165.3 %all-gather.7.cloned.1.call-start = ((), (), s32[]{:S(2)}) async-start(), calls=%async_computation.11 | async-start | bytes 5242880 | tf_op jit(solution)/shard_map/all_gather | solution.py:107
  83.4 67.2 %all-to-all-start.1 = ((bf16[512,4,352]{0,2,1:T(8,128)(2,1)}), bf16[512,4,352]{0,2,1:T(8,128)(2,1)S(1)}, u32[]{:S(2)}, u32[]{:S(2)}) async-start(bf16[512,4,352]{0,2,1:T(8,128)(2,1)} %bitcast.40), calls=%async_computation.1 | async-start | bytes 2883584 | tf_op jit(solution)/shard_map/all_to_all | solution.py:93
  150.7 37.5 %all-to-all-start.2 = ((bf16[4,352,512]{2,1,0:T(8,128)(2,1)}), bf16[4,352,512]{2,1,0:T(8,128)(2,1)}, u32[]{:S(2)}, u32[]{:S(2)}) async-start(bf16[4,352,512]{2,1,0:T(8,128)(2,1)} %bitcast.37), calls=%async_computation.2 | async-start | bytes 2883584 | tf_op jit(solution)/shard_map/all_to_all | solution.py:97
  155.2 93.4 %reduce-scatter.5.cloned.1.call-start = ((), (), s32[]{:S(2)}) async-start(), calls=%async_computation.12 | async-start | bytes 5242880 | tf_op jit(solution)/shard_map/reduce_scatter | solution.py:112
  188.2 2.8 copy-start.2
  205.0 43.8 %copy-start.5 = (f32[512]{0:T(512)S(1)}, f32[512]{0:T(512)}, u32[]{:S(2)}) copy-start(f32[512]{0:T(512)} %param.22) | copy-start | bytes 6148
  205.0 73.2 %copy-start.1 = (bf16[256,512]{1,0:T(8,128)(2,1)S(1)}, bf16[256,512]{1,0:T(8,128)(2,1)}, u32[]{:S(2)}) copy-start(bf16[256,512]{1,0:T(8,128)(2,1)} %param.15) | copy-start | bytes 786436
  205.0 81.3 %copy-start = (f32[512,1408]{1,0:T(8,128)S(1)}, f32[512,1408]{1,0:T(8,128)}, u32[]{:S(2)}) copy-start(f32[512,1408]{1,0:T(8,128)} %param.24) | copy-start | bytes 8650756
  205.0 80.4 %copy-start.4 = (f32[512]{0:T(512)S(1)}, f32[512]{0:T(512)}, u32[]{:S(2)}) copy-start(f32[512]{0:T(512)} %param.23) | copy-start | bytes 6148
  205.0 73.1 %reduce-scatter.7.cloned.1.call-start = ((), (), s32[]{:S(2)}) async-start(), calls=%async_computation.13 | async-start | bytes 1310720 | tf_op jit(solution)/shard_map/reduce_scatter | solution.py:113
  248.7 52.7 %all-gather.9.cloned.1.call-start = ((), (), s32[]{:S(2)}) async-start(), calls=%async_computation.14 | async-start | bytes 1310720 | tf_op jit(solution)/shard_map/all_gather | solution.py:14
  288.0 62.3 %all-to-all-start.3 = ((bf16[512,4,352]{0,2,1:T(8,128)(2,1)}), bf16[512,4,352]{0,2,1:T(8,128)(2,1)S(1)}, u32[]{:S(2)}, u32[]{:S(2)}) async-start(bf16[512,4,352]{0,2,1:T(8,128)(2,1)} %bitcast.6), calls=%async_computation.5 | async-start | bytes 2883584 | tf_op jit(solution)/shard_map/all_to_all | solution.py:93
  291.6 166.3 %all-gather.11.cloned.1.call-start = ((), (), s32[]{:S(2)}) async-start(), calls=%async_computation.15 | async-start | bytes 5242880 | tf_op jit(solution)/shard_map/all_gather | solution.py:107
  350.3 67.2 %all-to-all-start.4 = ((bf16[512,4,352]{0,2,1:T(8,128)(2,1)}), bf16[512,4,352]{0,2,1:T(8,128)(2,1)S(1)}, u32[]{:S(2)}, u32[]{:S(2)}) async-start(bf16[512,4,352]{0,2,1:T(8,128)(2,1)} %bitcast.41), calls=%async_computation.6 | async-start | bytes 2883584 | tf_op jit(solution)/shard_map/all_to_all | solution.py:93
  417.5 37.5 %all-to-all-start.5 = ((bf16[4,352,512]{2,1,0:T(8,128)(2,1)}), bf16[4,352,512]{2,1,0:T(8,128)(2,1)}, u32[]{:S(2)}, u32[]{:S(2)}) async-start(bf16[4,352,512]{2,1,0:T(8,128)(2,1)} %bitcast.39), calls=%async_computation.7 | async-start | bytes 2883584 | tf_op jit(solution)/shard_map/all_to_all | solution.py:97
  421.8 93.6 %reduce-scatter.9.cloned.1.call-start = ((), (), s32[]{:S(2)}) async-start(), calls=%async_computation.16 | async-start | bytes 5242880 | tf_op jit(solution)/shard_map/reduce_scatter | solution.py:112
  455.0 2.8 copy-start.3
  471.8 43.6 %copy-start.6 = (f32[512]{0:T(512)S(1)}, f32[512]{0:T(512)}, u32[]{:S(2)}) copy-start(f32[512]{0:T(512)} %param.29) | copy-start | bytes 6148
  471.8 73.2 %reduce-scatter.11.cloned.1.call-start = ((), (), s32[]{:S(2)}) async-start(), calls=%async_computation.17 | async-start | bytes 1310720 | tf_op jit(solution)/shard_map/reduce_scatter | solution.py:113
Sparse Core Ops, SparseCore 0:
  18.0 16.9 all-gather.4
  36.6 127.9 all-gather.6
  205.1 43.4 reduce-scatter.4
  250.8 27.2 reduce-scatter.6
  286.4 14.9 all-gather.8
  302.8 128.8 all-gather.10
  472.0 43.3 reduce-scatter.8
  517.7 27.2 reduce-scatter.10

commit v2 on v0

--- a/solution.py
+++ b/solution.py
@@ -1,7 +1,13 @@
+import functools
+
 import jax
 import jax.numpy as jnp
 from jax import lax
+from jax.experimental import pallas as pl
+from jax.experimental.pallas import tpu as pltpu
 from jax.sharding import PartitionSpec as P
+
+MESH = pl.DeviceIdType.MESH
 
 epsilon = 1e-06
 
@@ -48,7 +54,7 @@
     return (values + 0.5 * summed * down_s).astype(jnp.bfloat16)
 
 
-def body(
+def body_gather(
     tokens,
     gain_first,
     gate_first,
@@ -89,6 +95,387 @@
     )
 
 
+def exchange_kernel(n_fs, *refs):
+    z_send, z_recv, x_send, x_recv, own_sem = refs[-5:]
+    count = (len(refs) - 5) // 3
+    sources, results, held = (refs[i * count : (i + 1) * count] for i in range(3))
+    grp, fs = lax.axis_index("grp"), lax.axis_index("fs")
+    partner = {"grp": 1 - grp}
+    peers = [lax.rem(fs + d, n_fs) for d in range(n_fs)]
+    origins = [lax.rem(fs + n_fs - d, n_fs) for d in range(n_fs)]
+
+    barrier = pltpu.get_barrier_semaphore()
+    for d in range(1, n_fs):
+        pl.semaphore_signal(barrier, inc=1, device_id={"fs": peers[d]}, device_id_type=MESH)
+    pl.semaphore_signal(barrier, inc=1, device_id=partner, device_id_type=MESH)
+    pl.semaphore_wait(barrier, n_fs)
+
+    def my_half(ref):
+        half = ref.shape[1] // 2
+        return pl.ds(grp * half, half)
+
+    def along_z(m, d):
+        rows = my_half(sources[m])
+        return pltpu.make_async_remote_copy(
+            src_ref=sources[m].at[peers[d], rows],
+            dst_ref=results[m].at[fs, rows],
+            send_sem=z_send.at[m, d - 1],
+            recv_sem=z_recv.at[m, d - 1],
+            device_id={"fs": peers[d]},
+            device_id_type=MESH,
+        )
+
+    def along_x(m, d):
+        block = results[m].at[origins[d], my_half(results[m])]
+        return pltpu.make_async_remote_copy(
+            src_ref=block,
+            dst_ref=block,
+            send_sem=x_send.at[m, d - 1],
+            recv_sem=x_recv.at[m, d - 1],
+            device_id=partner,
+            device_id_type=MESH,
+        )
+
+    order = [(m, d) for m in range(count) for d in range(1, n_fs)]
+    for m, d in order:
+        along_z(m, d).start()
+    loads = [pltpu.make_async_copy(sources[m].at[fs], held[m], own_sem.at[m]) for m in range(count)]
+    stores = [pltpu.make_async_copy(held[m], results[m].at[fs], own_sem.at[m]) for m in range(count)]
+    for load in loads:
+        load.start()
+    for load, store in zip(loads, stores):
+        load.wait()
+        store.start()
+    for m, d in order:
+        along_z(m, d).wait_recv()
+        along_x(m, d).start()
+    for store in stores:
+        store.wait()
+    for m, d in order:
+        along_z(m, d).wait_send()
+        along_x(m, d).wait()
+
+
+def column_chunks(weight):
+    n = lax.axis_size("fs")
+    parts = weight.astype(jnp.bfloat16).reshape(weight.shape[0], n, -1).transpose(1, 0, 2)
+    return jnp.pad(parts, ((0, 0), (0, 0), (0, -parts.shape[2] % 128)))
+
+
+def row_chunks(weight):
+    return weight.astype(jnp.bfloat16).reshape(lax.axis_size("fs"), -1, weight.shape[1])
+
+
+def exchange(which, arrays):
+    n, count = lax.axis_size("fs"), len(arrays)
+    any_spec = pl.BlockSpec(memory_space=pl.ANY)
+    return pl.pallas_call(
+        functools.partial(exchange_kernel, n),
+        out_shape=[jax.ShapeDtypeStruct(a.shape, a.dtype) for a in arrays],
+        in_specs=[any_spec] * count,
+        out_specs=[any_spec] * count,
+        scratch_shapes=[pltpu.VMEM(a.shape[1:], a.dtype) for a in arrays]
+        + [pltpu.SemaphoreType.DMA((count, n - 1))] * 4
+        + [pltpu.SemaphoreType.DMA((count,))],
+        compiler_params=pltpu.CompilerParams(collective_id=which, has_side_effects=True),
+        cost_estimate=pl.CostEstimate(
+            flops=2 * 10**9 * count,
+            bytes_accessed=4 * sum(a.size for a in arrays),
+            transcendentals=0,
+        ),
+    )(*arrays)
+
+
+def own_columns(scale):
+    width = scale.shape[0] // lax.axis_size("fs")
+    return lax.dynamic_slice_in_dim(scale, lax.axis_index("fs") * width, width)
+
+
+def gather_kernel(n_fs, n_tp, block, out, held, own_sem, z_send, z_recv, y_send, y_recv, c_send, c_recv):
+    fs, tp = lax.axis_index("fs"), lax.axis_index("tp")
+    chips = n_tp // 2
+    core = {"tp": tp + 1 - 2 * lax.rem(tp, 2)}
+    peers = [lax.rem(fs + d, n_fs) for d in range(n_fs)]
+    origins = [lax.rem(fs + n_fs - d, n_fs) for d in range(n_fs)]
+    across = [lax.rem(tp + 2 * k, n_tp) for k in range(chips)]
+    came_from = [lax.rem(tp + n_tp - 2 * k, n_tp) for k in range(chips)]
+
+    barrier = pltpu.get_barrier_semaphore()
+    greeted = [{"fs": p} for p in peers[1:]] + [{"tp": p} for p in across[1:]] + [core]
+    for device in greeted:
+        pl.semaphore_signal(barrier, inc=1, device_id=device, device_id_type=MESH)
+    pl.semaphore_wait(barrier, len(greeted))
+
+    def send(src, slot, sends, recvs, device):
+        return pltpu.make_async_remote_copy(
+            src_ref=src,
+            dst_ref=out.at[slot],
+            send_sem=sends,
+            recv_sem=recvs,
+            device_id=device,
+            device_id_type=MESH,
+        )
+
+    def along_z(d):
+        return send(block, (fs, tp), z_send.at[d], z_recv.at[d], {"fs": peers[d]})
+
+    def along_y(d, k):
+        src = block if d == 0 else out.at[origins[d], tp]
+        return send(src, (origins[d], tp), y_send.at[d, k], y_recv.at[d, k], {"tp": across[k]})
+
+    def to_core(d, k):
+        slot = (origins[d], came_from[k])
+        src = block if d == 0 and k == 0 else out.at[slot]
+        return send(src, slot, c_send.at[d, k], c_recv.at[d, k], core)
+
+    def pass_on(d):
+        for k in range(1, chips):
+            along_y(d, k).start()
+        to_core(d, 0).start()
+
+    def share(d):
+        for k in range(1, chips):
+            along_y(d, k).wait_recv()
+            to_core(d, k).start()
+
+    for d in range(1, n_fs):
+        along_z(d).start()
+    pass_on(0)
+    load = pltpu.make_async_copy(block, held, own_sem)
+    load.start()
+    load.wait()
+    store = pltpu.make_async_copy(held, out.at[fs, tp], own_sem)
+    store.start()
+    for d in range(1, n_fs):
+        along_z(d).wait_recv()
+        pass_on(d)
+        share(d - 1)
+    share(n_fs - 1)
+    store.wait()
+    for d in range(n_fs):
+        if d > 0:
+            along_z(d).wait_send()
+        for k in range(chips):
+            if k > 0:
+                along_y(d, k).wait_send()
+            to_core(d, k).wait()
+
+
+def gather_tokens(which, stream):
+    n_fs, n_tp = lax.axis_size("fs"), lax.axis_size("tp")
+    any_spec = pl.BlockSpec(memory_space=pl.ANY)
+    dma = pltpu.SemaphoreType.DMA
+    whole = pl.pallas_call(
+        functools.partial(gather_kernel, n_fs, n_tp),
+        out_shape=jax.ShapeDtypeStruct((n_fs, n_tp, *stream.shape), stream.dtype),
+        in_specs=[any_spec],
+        out_specs=any_spec,
+        scratch_shapes=[pltpu.VMEM(stream.shape, stream.dtype), dma(())]
+        + [dma((n_fs,))] * 2
+        + [dma((n_fs, n_tp // 2))] * 4,
+        compiler_params=pltpu.CompilerParams(collective_id=which, has_side_effects=True),
+        cost_estimate=pl.CostEstimate(
+            flops=10**9, bytes_accessed=stream.size * 32, transcendentals=0
+        ),
+    )(stream)
+    return whole.transpose(0, 2, 1, 3).reshape(n_fs * stream.shape[0], -1)
+
+
+def scatter_kernel(
+    n_fs, n_tp, terms, stream, scale, out, from_core, summed, from_y, total, from_z, acc,
+    c_send, c_recv, y_send, y_recv, z_send, z_recv
+):
+    fs, tp = lax.axis_index("fs"), lax.axis_index("tp")
+    chips = n_tp // 2
+    flip = 1 - 2 * lax.rem(tp, 2)
+    core = {"tp": tp + flip}
+    peers = [lax.rem(fs + d, n_fs) for d in range(n_fs)]
+    across = [lax.rem(tp + 2 * k, n_tp) for k in range(chips)]
+    order = list(range(1, n_fs)) + [0]
+    rows = stream.shape[0]
+    step = 64
+
+    barrier = pltpu.get_barrier_semaphore()
+    greeted = [{"fs": p} for p in peers[1:]] + [{"tp": p} for p in across[1:]] + [core]
+    for device in greeted:
+        pl.semaphore_signal(barrier, inc=1, device_id=device, device_id_type=MESH)
+    pl.semaphore_wait(barrier, len(greeted))
+
+    def send(src, dst, sends, recvs, device):
+        return pltpu.make_async_remote_copy(
+            src_ref=src,
+            dst_ref=dst,
+            send_sem=sends,
+            recv_sem=recvs,
+            device_id=device,
+            device_id_type=MESH,
+        )
+
+    def to_core(d, k):
+        src = terms.at[across[k] + flip, peers[d]]
+        return send(src, from_core.at[d, k], c_send.at[d, k], c_recv.at[d, k], core)
+
+    def along_y(d, k):
+        return send(
+            summed.at[d, k], from_y.at[d, k], y_send.at[d, k], y_recv.at[d, k], {"tp": across[k]}
+        )
+
+    def along_z(d):
+        return send(total.at[d], from_z.at[d], z_send.at[d], z_recv.at[d], {"fs": peers[d]})
+
+    def combine(dst, parts):
+        def one(i, carry):
+            piece = pl.ds(i * step, step)
+            value = parts[0][piece].astype(jnp.float32)
+            for part in parts[1:]:
+                value = value + part[piece].astype(jnp.float32)
+            dst[piece] = value.astype(dst.dtype)
+            return carry
+
+        lax.fori_loop(0, rows // step, one, 0)
+
+    for d in order:
+        for k in reversed(range(chips)):
+            to_core(d, k).start()
+    for d in order:
+        for k in reversed(range(chips)):
+            to_core(d, k).wait_recv()
+            if k > 0:
+                combine(summed.at[d, k], [terms.at[across[k], peers[d]], from_core.at[d, k]])
+                along_y(d, k).start()
+    for d in order:
+        for k in range(1, chips):
+            along_y(d, k).wait_recv()
+        parts = [terms.at[tp, peers[d]], from_core.at[d, 0]]
+        parts = parts + [from_y.at[d, k] for k in range(1, chips)]
+        combine(acc if d == 0 else total.at[d], parts)
+        if d > 0:
+            along_z(d).start()
+    for d in range(1, n_fs):
+        along_z(d).wait_recv()
+
+    def finish_rows(i, carry):
+        piece = pl.ds(i * step, step)
+        value = acc[piece]
+        for d in range(1, n_fs):
+            value = value + from_z[d, piece].astype(jnp.float32)
+        value = stream[piece].astype(jnp.float32) + 0.5 * value * scale[...]
+        out[piece] = value.astype(out.dtype)
+        return carry
+
+    lax.fori_loop(0, rows // step, finish_rows, 0)
+    for d in range(n_fs):
+        if d > 0:
+            along_z(d).wait_send()
+        for k in range(chips):
+            if k > 0:
+                along_y(d, k).wait_send()
+            to_core(d, k).wait_send()
+
+
+def scatter_finish(which, terms, stream, scale):
+    n_fs, n_tp = lax.axis_size("fs"), lax.axis_size("tp")
+    chips = n_tp // 2
+    tile = stream.shape
+    vmem = pl.BlockSpec(memory_space=pltpu.VMEM)
+    dma = pltpu.SemaphoreType.DMA
+    half = jnp.bfloat16
+    return pl.pallas_call(
+        functools.partial(scatter_kernel, n_fs, n_tp),
+        out_shape=jax.ShapeDtypeStruct(tile, half),
+        in_specs=[vmem] * 3,
+        out_specs=vmem,
+        scratch_shapes=[
+            pltpu.VMEM((n_fs, chips, *tile), half),
+            pltpu.VMEM((n_fs, chips, *tile), half),
+            pltpu.VMEM((n_fs, chips, *tile), half),
+            pltpu.VMEM((n_fs, *tile), half),
+            pltpu.VMEM((n_fs, *tile), half),
+            pltpu.VMEM(tile, jnp.float32),
+        ]
+        + [dma((n_fs, chips))] * 4
+        + [dma((n_fs,))] * 2,
+        compiler_params=pltpu.CompilerParams(collective_id=which, has_side_effects=True),
+        cost_estimate=pl.CostEstimate(
+            flops=10**9, bytes_accessed=2 * terms.size, transcendentals=0
+        ),
+    )(terms.reshape(n_tp, n_fs, *tile), stream, scale[None, :])
+
+
+def block(n, stream, gain, weights, gate_s, up_s, down_s, later):
+    gate_w, up_w, down_w = weights
+    every = gather_tokens(3 + n, stream).astype(jnp.float32)
+    mean = jnp.mean(every * every, axis=1, keepdims=True)
+    normed = (every * lax.rsqrt(mean + epsilon) * gain).astype(jnp.bfloat16)
+    width = down_w.shape[1]
+
+    def project(weight, scale):
+        wide = jnp.dot(
+            normed, weight.reshape(-1, weight.shape[2]), preferred_element_type=jnp.float32
+        )
+        return wide[:, :width] * own_columns(scale)
+
+    hidden = (jax.nn.silu(project(gate_w, gate_s)) * project(up_w, up_s)).astype(jnp.bfloat16)
+    terms = jnp.stack(
+        [
+            jnp.dot(hidden, w, preferred_element_type=jnp.float32).astype(jnp.bfloat16)
+            for w in down_w
+        ]
+    )
+    if not later:
+        return scatter_finish(6, terms, stream, down_s), later
+    terms, later = lax.optimization_barrier((terms, later))
+    mine = lax.psum_scatter(terms, "tp", scatter_dimension=0, tiled=False)
+    summed = lax.psum_scatter(mine, "fs", scatter_dimension=0, tiled=True)
+    out = stream.astype(jnp.float32) + 0.5 * summed.astype(jnp.float32) * down_s
+    return out.astype(jnp.bfloat16), later
+
+
+def body_exchange(
+    tokens,
+    gain_first,
+    gate_first,
+    gate_scale_first,
+    up_first,
+    up_scale_first,
+    down_first,
+    down_scale_first,
+    gain_second,
+    gate_second,
+    gate_scale_second,
+    up_second,
+    up_scale_second,
+    down_second,
+    down_scale_second,
+):
+    gains = lax.all_gather(jnp.stack([gain_first, gain_second]), "tp", axis=1, tiled=True)
+    columns = exchange(0, [column_chunks(gate_first), column_chunks(up_first)])
+    rows = exchange(1, [row_chunks(down_first)])
+    later = ([column_chunks(gate_second), column_chunks(up_second)], [row_chunks(down_second)])
+    middle, later = block(
+        1,
+        tokens,
+        gains[0],
+        (*columns, *rows),
+        gate_scale_first,
+        up_scale_first,
+        down_scale_first,
+        later,
+    )
+    columns = exchange(2, later[0])
+    rows = exchange(3, later[1])
+    return block(
+        2,
+        middle,
+        gains[1],
+        (*columns, *rows),
+        gate_scale_second,
+        up_scale_second,
+        down_scale_second,
+        (),
+    )[0]
+
+
 def solution(mesh):
     in_specs = (
         P(("grp", "fs"), "tp"),
@@ -108,4 +495,12 @@
         P("tp"),
     )
     out_specs = P(("grp", "fs"), "tp")
+
+    def body(*args):
+        n_fs, n_tp = lax.axis_size("fs"), lax.axis_size("tp")
+        width = args[2].shape[1] // n_fs
+        fits = width >= 128 and width % 32 == 0 and n_fs == n_tp and n_tp % 2 == 0 and lax.axis_size("grp") == 2
+        fits = fits and args[0].shape[0] % 64 == 0
+        return (body_exchange if fits else body_gather)(*args)
+
     return jax.shard_map(body, mesh=mesh, in_specs=in_specs, out_specs=out_specs, check_vma=False)

time: 770 us -> 427 us (0.55)
  waiting for transfers between devices: 691 us -> 49.3 us
  Pallas kernels: 0 us -> 281 us
  local copies, waits for them, and re-layouts: 0.66 us -> 37.8 us
  matrix products: 29.2 us -> 20.2 us
  blocking collectives: 14.2 us -> 5.21 us
    all_gather x8 -> x0, waiting for transfers between devices: 646 us -> none  [the longest x2 213 us: collect_down(): lax.all_gather(down_w.astype(jnp.bfloat16), 'fs', axis=1, tiled=True)]
    pallas_call x0 -> x7, Pallas kernels: none -> 281 us  [the longest x4 159 us: exchange(): pl.pallas_call(functools.partial(exchange_kernel, n), out_shape=[jax.Shap...]
    unnamed x24 -> x41, local copies, waits for them, and re-layouts: 0.66 us -> 18.4 us
    psum x2 -> x0, blocking collectives: 14.2 us -> none  [normalize(): totals = lax.psum(jnp.sum(values * values, axis=1), 'tp')]
    convert_element_type x9 -> x5, other arithmetic: 18.1 us -> 8.34 us  [the longest x2 4.56 us: row_chunks(): weight.astype(jnp.bfloat16)]
    dot_general x4 -> x12, matrix products: 29.2 us -> 20.2 us  [the longest x4 10.2 us: project(): jnp.dot(normed, weight.reshape(-1, weight.shape[2]), preferred_element_ty...]
  transfers between devices with their start and end apart: 10 -> 2, of which waited for: 10 -> 1; matrix products, arithmetic and copies ran while one was open for 3% -> 0% of each run, Pallas kernels for 0% -> 19%
where the time goes in v2:
time: 427 us; the launch traced here: 426 us
  Pallas kernels  281 us (66%)
  waiting for transfers between devices  49.3 us (12%)
  local copies, waits for them, and re-layouts  37.8 us (9%)
  matrix products  20.2 us (5%)
  other arithmetic  19.2 us (4%)
  between operations  13.8 us (3%)
  blocking collectives  5.21 us (1%)
    pallas_call x4, Pallas kernels, exchange(): pl.pallas_call(functools.partial(exchange_kernel, n), out_shape=[jax.Shap...  159 us
    pallas_call x2, Pallas kernels, gather_tokens(): pl.pallas_call(functools.partial(gather_kernel, n_fs, n_tp), out_shape=ja...  77.1 us
    reduce_scatter x1, waiting for transfers between devices, block(): mine = lax.psum_scatter(terms, 'tp', scatter_dimension=0, tiled=False)  49.2 us
    pallas_call x1, Pallas kernels, scatter_finish(): pl.pallas_call(functools.partial(scatter_kernel, n_fs, n_tp), out_shape=j...  44.6 us
    unnamed x41, local copies, waits for them, and re-layouts  18.4 us
    dot_general x4, matrix products, project(): jnp.dot(normed, weight.reshape(-1, weight.shape[2]), preferred_element_ty...  10.2 us
    dot_general x8, matrix products, block(): jnp.dot(hidden, w, preferred_element_type=jnp.float32).astype(jnp.bfloat16)  10.1 us
  transfers between devices with their start and end apart: 2, of which 1 were waited for; matrix products, arithmetic and copies ran while one was open for 0% of the time, Pallas kernels for 19%

profile of v2, /device:TPU:0, one launch (start us, length us, event | category | flops | bytes accessed | tf_op | source)
XLA Modules:
  0.0 426.3 jit_solution(12463948035102141142)
XLA Ops:
  6.5 38.7 %shard_map.145 = bf16[4,4,256,512]{3,2,1,0:T(8,128)(2,1)} custom-call(bf16[256,512]{1,0:T(8,128)(2,1)} %block.1), custom_call_target="tpu_custom_call" | custom-call | flops 1000000000 | bytes 4194304 | tf_op jit(solution)/shard_map/pallas_call | solution.py:268
  45.3 5.2 %all_gather.3 = f32[2,2048]{1,0:T(2,128)S(1)} all-gather(f32[2,512]{1,0:T(2,128)S(1)} %pad_maximum_fusion.2), channel_id=1, replica_groups=mesh['grp'=2,'fs'=4,'tp'=4] {'tp'}, dimensions={1}, use_global_device_ids=true | all-gather | bytes 20480 | tf_op jit(solution)/shard_map/all_gather | solution.py:451
  50.6 3.2 fusion
  53.8 0.2 copy-done
  54.0 1.0 fusion.7
  55.1 3.2 copy.16
  58.3 3.3 copy.26
  61.6 2.1 copy.17
  63.7 0.9 copy.18
  64.6 3.0 copy.19
  67.5 1.8 copy.20
  69.4 1.3 pad.13.refs_0_
  70.7 1.4 pad.14.refs_1_
  72.1 0.8 dynamic_slice.12
  72.9 0.8 dynamic_slice.13
  73.6 3.2 convert_element_type.104
  76.8 31.1 %shard_map.147 = bf16[4,352,512]{2,1,0:T(8,128)(2,1)} custom-call(bf16[4,352,512]{2,1,0:T(8,128)(2,1)} %bitcast.91), custom_call_target="tpu_custom_call" | custom-call | flops 2000000000 | bytes 2883584 | tf_op jit(solution)/shard_map/pallas_call | solution.py:172
  108.0 45.0 %shard_map.146 = (bf16[4,512,384]{2,1,0:T(8,128)(2,1)}, bf16[4,512,384]{2,1,0:T(8,128)(2,1)}) custom-call(bf16[4,512,384]{2,1,0:T(8,128)(2,1)} %pad.13.refs_0_, bf16[4,512,384]{2,1,0:T(8,128)(2,1)} %pad.14.refs_1_), custom_call_target="tpu_custom_call" | custom-call | flops 4000000000 | bytes 6291456 | tf_op jit(solution)/shard_map/pallas_call | solution.py:172
  153.0 4.5 %fusion.16 = f32[1024,352]{0,1:T(8,128)S(1)} fusion(bf16[1024,2048]{1,0:T(8,128)(2,1)} %bitcast.86, bf16[2048,384]{1,0:T(8,128)(2,1)} %bitcast.103, f32[352]{0:T(512)S(1)} %dynamic_slice.12), kind=kOutput, calls=%fused_computation.30 | convolution fusion | flops 1476755456 | bytes 7210368 | tf_op jit(solution)/shard_map/dot_general | solution.py:413
  157.6 1.9 fusion.37
  159.5 1.7 fusion.43
  161.3 1.8 fusion.42
  163.1 1.7 fusion.41
  164.8 1.7 fusion.40
  166.5 2.1 copy.21
  168.6 0.9 copy.22
  169.5 1.3 pad.15.refs_0_
  170.8 2.1 copy.23
  172.9 0.9 copy.24
  173.8 0.0 copy-start.3
  173.8 1.4 pad.16.refs_1_
  175.2 1.0 copy-done.3
  176.2 1.4 convert_element_type.111
  177.6 0.1 copy-done.5
  177.7 0.6 copy-done.6
  178.3 0.3 copy-done.7
  178.6 0.3 copy-done.8
  178.9 2.2 pad_maximum_fusion
  181.1 0.0 reduce-scatter.3.cloned.1.call-update
  181.1 0.3 reduce-scatter.5.cloned.1.call-start
  181.4 49.2 %reduce-scatter.3.cloned.1.call-done = bf16[1,1024,512]{2,1,0:T(8,128)(2,1)} async-done(((bf16[4,1024,512]{2,1,0:T(8,128)(2,1)}), bf16[1,1024,512]{2,1,0:T(8,128)(2,1)}) %reduce-scatter.3.cloned.1.call-update) | async-done | bytes 1048592 | tf_op jit(solution)/shard_map/reduce_scatter | solution.py:428
  230.6 0.0 reduce-scatter.5.cloned.1.call-update
  230.6 0.8 dynamic_slice.14
  231.4 0.8 dynamic_slice.15
  232.2 33.8 %shard_map.150 = bf16[4,352,512]{2,1,0:T(8,128)(2,1)} custom-call(bf16[4,352,512]{2,1,0:T(8,128)(2,1)} %bitcast.90), custom_call_target="tpu_custom_call" | custom-call | flops 2000000000 | bytes 2883584 | tf_op jit(solution)/shard_map/pallas_call | solution.py:172
  266.0 0.0 copy-start.4
  266.0 48.8 %shard_map.149 = (bf16[4,512,384]{2,1,0:T(8,128)(2,1)}, bf16[4,512,384]{2,1,0:T(8,128)(2,1)}) custom-call(bf16[4,512,384]{2,1,0:T(8,128)(2,1)} %pad.15.refs_0_, bf16[4,512,384]{2,1,0:T(8,128)(2,1)} %pad.16.refs_1_), custom_call_target="tpu_custom_call" | custom-call | flops 4000000000 | bytes 6291456 | tf_op jit(solution)/shard_map/pallas_call | solution.py:172
  314.8 0.0 reduce-scatter.5.cloned.1.call-done
  314.9 1.7 add_convert_fusion.block.stream
  316.6 38.4 %shard_map.148 = bf16[4,4,256,512]{3,2,1,0:T(8,128)(2,1)} custom-call(bf16[256,512]{1,0:T(8,128)(2,1)} %add_convert_fusion.block.stream), custom_call_target="tpu_custom_call" | custom-call | flops 1000000000 | bytes 4194304 | tf_op jit(solution)/shard_map/pallas_call | solution.py:268
  355.0 3.2 fusion.3
  358.3 0.2 copy-done.1
  358.5 1.0 fusion.6
  359.5 3.2 copy.25
  362.7 1.4 copy.27
  364.2 1.8 fusion.25
  366.0 1.9 fusion.34
  367.9 0.8 convolution_convert_fusion
  368.7 0.8 convolution_convert_fusion.1
  369.5 0.8 convolution_convert_fusion.2
  370.2 0.8 convolution_convert_fusion.3
  371.0 2.2 pad_maximum_fusion.1.terms
  373.2 44.6 %shard_map.151 = bf16[256,512]{1,0:T(8,128)(2,1)} custom-call(bf16[4,4,256,512]{3,2,1,0:T(8,128)(2,1)} %pad_maximum_fusion.1.terms, bf16[256,512]{1,0:T(8,128)(2,1)} %add_convert_fusion.block.stream, f32[1,512]{1,0:T(1,128)} %bitcast.97), custom_call_target="tpu_custom_call" | custom-call | flops 1000000000 | bytes 4194304 | tf_op jit(solution)/shard_map/pallas_call | solution.py:383
  417.8 1.7 copy.29
  (33 shorter events, 0.1 us)
Async XLA Ops:
  6.5 224.1 %reduce-scatter.3.cloned.1.call-start = ((), (), s32[]{:S(2)}) async-start(), calls=%async_computation.2 | async-start | bytes 5242880 | tf_op jit(solution)/shard_map/reduce_scatter | solution.py:428
  6.5 38.8 %copy-start.10 = (f32[512]{0:T(512)S(1)}, f32[512]{0:T(512)}, u32[]{:S(2)}) copy-start(f32[512]{0:T(512)} %param.23) | copy-start | bytes 6148
  6.5 38.8 %copy-start.11 = (f32[512]{0:T(512)S(1)}, f32[512]{0:T(512)}, u32[]{:S(2)}) copy-start(f32[512]{0:T(512)} %param.16) | copy-start | bytes 6148
  50.6 3.5 copy-start
  153.0 4.5 %copy-start.2 = (bf16[128,8,4,512]{3,1,2,0:T(8,128)(2,1)S(1)}, bf16[128,8,4,512]{3,1,2,0:T(8,128)(2,1)}, u32[]{:S(2)}) copy-start(bf16[128,8,4,512]{3,1,2,0:T(8,128)(2,1)} %copy.26) | copy-start | bytes 12582916
  153.0 4.5 %copy-start.14 = (bf16[4,512,384]{2,1,0:T(8,128)(2,1)S(1)}, bf16[4,512,384]{2,1,0:T(8,128)(2,1)}, u32[]{:S(2)}) copy-start(bf16[4,512,384]{2,1,0:T(8,128)(2,1)} %get-tuple-element.14) | copy-start | bytes 4718596
  157.6 2.0 copy-start.15
  173.8 2.4 copy-start.3
  176.2 1.5 copy-start.5
  176.2 2.1 copy-start.6
  176.2 2.4 copy-start.7
  176.2 2.7 copy-start.8
  181.1 133.8 %reduce-scatter.5.cloned.1.call-start = ((), (), s32[]{:S(2)}) async-start(), calls=%async_computation.3 | async-start | bytes 1310720 | tf_op jit(solution)/shard_map/reduce_scatter | solution.py:429
  232.2 33.8 %copy-start.9 = (f32[512]{0:T(512)S(1)}, f32[512]{0:T(512)}, u32[]{:S(2)}) copy-start(f32[512]{0:T(512)} %param.22) | copy-start | bytes 6148
  266.0 48.9 %copy-start.4 = (bf16[256,512]{1,0:T(8,128)(2,1)S(1)}, bf16[256,512]{1,0:T(8,128)(2,1)}, u32[]{:S(2)}) copy-start(bf16[256,512]{1,0:T(8,128)(2,1)} %block.1) | copy-start | bytes 786436
  355.0 3.5 copy-start.1
  362.7 1.4 copy-start.13
  364.2 1.8 copy-start.12
  366.0 2.0 copy-start.16
Sparse Core Ops, SparseCore 0:
  181.2 49.3 reduce-scatter.2
  232.9 35.1 reduce-scatter.4
